TPU v7x, 256 devices: a whole 4x4x8 slice. The times are simulated.
256 devices in a mesh: ep: 32 (over z, x), tp: 8 (over y, core).
Axes of the slice: x: 4, y: 4, z: 8, core: 2. Of those that a mesh axis runs over, the one named last changes fastest.
Arguments:
- resid: bfloat16 [1024, 2048], P('ep'), may hold values from -6 to 6
- norm_gain: bfloat16 [2048], replicated, may hold values from 0.099609375 to 1.8984375
- w_query: bfloat16 [2048, 1024], P(None, 'tp'), may hold values from -0.125 to 0.125
- w_key: bfloat16 [2048, 1024], P(None, 'tp'), may hold values from -0.125 to 0.125
- w_value: bfloat16 [2048, 1024], P(None, 'tp'), may hold values from -0.125 to 0.125
- w_gate: bfloat16 [2048, 1024], P(None, 'tp'), may hold values from -0.125 to 0.125
- head_gain: bfloat16 [1024], P('tp'), may hold values from 0.099609375 to 1.8984375
- w_output: bfloat16 [1024, 2048], P('tp'), may hold values from -0.1875 to 0.1875
- state: float32 [1024, 8, 128, 128], P('ep', 'tp'), may hold values from -0.6 to 0.6
- positions: int32 [1024], P('ep'), may hold values from 1024 to 8191
- ffn_gain: bfloat16 [2048], replicated, may hold values from 0.099609375 to 1.8984375
- w_mix: bfloat16 [2048], replicated, may hold values from -0.125 to 0.125
- dense_gate: bfloat16 [2048, 5632], P('tp', 'ep'), may hold values from -0.125 to 0.125
- dense_up: bfloat16 [2048, 5632], P('tp', 'ep'), may hold values from -0.125 to 0.125
- dense_down: bfloat16 [5632, 2048], P('ep', 'tp'), may hold values from -0.15625 to 0.15625
- routes: int32 [1024, 2], P('ep'), may hold values from 0 to 31, all different within a row; in each aligned block of 32 rows (0 to 31, 32 to 63, ...) at most 4 rows name the same one
- route_weight: bfloat16 [1024, 2], P('ep'), may hold values from 0.19921875 to 1
- expert_gate: bfloat16 [32, 2048, 4096], P('ep', None, 'tp'), may hold values from -0.125 to 0.125
- expert_up: bfloat16 [32, 2048, 4096], P('ep', None, 'tp'), may hold values from -0.125 to 0.125
- expert_down: bfloat16 [32, 4096, 2048], P('ep', 'tp'), may hold values from -0.09375 to 0.09375
Outputs:
- final: bfloat16 [1024, 2048], P('ep', 'tp')
- new_state: float32 [1024, 8, 128, 128], P('ep', 'tp')
Inputs may be any that keep to these rules, and one draw needn't show every extreme that they name: `routes`: each row names 2 different experts; in the rows of one index of ep no expert is named by more than 4 rows, a bound that some block reaches; every expert is named by some row.
All inputs are finite; a program needn't handle non-finite values.
Results may differ from a plain program's by a relative error of at most 0.018.
Values may be sent and summed in bfloat16 or wider, within the bound.
No kernel may reach another device: no remote copies, remote signals or barrier semaphores. Data moves between devices by JAX's collectives and lax.ppermute only.
A program may use at most 64 MiB of HBM per device.

v0:
```python
import jax
import jax.numpy as jnp
from jax import lax
from jax.sharding import PartitionSpec as P

EPSILON = 1e-06
THETA = 10000.0


def split_up(value, dim, length):
    before, after = (value.shape[:dim], value.shape[dim + 1 :])
    return jnp.moveaxis(value.reshape(*before, length, -1, *after), dim, 0)


def sent_and_summed(value, axis, dim):
    tiles = split_up(value, dim, lax.axis_size(axis))
    arrived = lax.all_to_all(tiles, axis, split_axis=0, concat_axis=0, tiled=True)
    return arrived.astype(jnp.float32).sum(axis=0)


def copy_for_each(value, axis):
    copies = jnp.broadcast_to(value, (lax.axis_size(axis), *value.shape))
    return lax.all_to_all(copies, axis, split_axis=0, concat_axis=0, tiled=True)


def of_everyone(value, axis):
    everything = copy_for_each(value, axis)
    return jnp.sum(everything.astype(jnp.float32), axis=0)


def in_order(tiles, dim):
    dims = list(tiles.shape[1:])
    dims[dim] *= tiles.shape[0]
    return jnp.moveaxis(tiles, 0, dim).reshape(dims)


def gather_directly(value, axis, dim):
    tiles = copy_for_each(value, axis)
    return in_order(tiles, dim)


def packed_total(arrays, axis):
    flat, at, outs = (jnp.concatenate([a.reshape(-1) for a in arrays]), 0, [])
    running = lax.psum(flat, axis)
    for a in arrays:
        outs.append(running[at : at + a.size].reshape(a.shape))
        at += a.size
    return tuple(outs)


def rms_norm(inputs, scaling):
    square = jnp.mean(inputs * inputs, axis=-1, keepdims=True)
    return inputs * lax.rsqrt(square + EPSILON) * scaling.astype(jnp.float32)


def rotate(inputs, places):
    halfway = inputs.shape[-1] // 2
    inverse = THETA ** (-jnp.arange(halfway, dtype=jnp.float32) / halfway)
    angles = places.astype(jnp.float32)[:, None] * inverse[None, :]
    cosine = jnp.cos(angles)[:, None, :]
    sine_of = jnp.sin(angles)[:, None, :]
    former = inputs[..., :halfway]
    latter = inputs[..., halfway:]
    return jnp.concatenate(
        [former * cosine - latter * sine_of, former * sine_of + latter * cosine], axis=-1
    )


def retain(queries, keys_in, values_in, gating, memory, places, head_first, head_gain):
    seqs_here = queries.shape[0]
    heads_here = memory.shape[1]
    head_size = memory.shape[2]
    head_shape = (seqs_here, heads_here, head_size)
    query_rot = rotate(queries.astype(jnp.float32).reshape(head_shape), places)
    key_rot = rotate(keys_in.astype(jnp.float32).reshape(head_shape), places) * head_size ** (-0.5)
    value_heads = values_in.astype(jnp.float32).reshape(head_shape)
    head_index = head_first + jnp.arange(heads_here, dtype=jnp.float32)
    decays = 1.0 - jnp.exp2(-1.0 - 1.5 * head_index)
    within = jnp.sum(query_rot * key_rot, axis=-1, keepdims=True) * value_heads
    carried = jnp.einsum("shd,shde->she", query_rot, memory) * decays[None, :, None]
    mixture = within + carried
    new_memory = (
        decays[None, :, None, None] * memory + key_rot[:, :, :, None] * value_heads[:, :, None, :]
    )
    centre = jnp.mean(mixture, axis=-1, keepdims=True)
    spread = jnp.mean(jnp.square(mixture - centre), axis=-1, keepdims=True)
    normed = ((mixture - centre) * lax.rsqrt(spread + EPSILON)).reshape(
        seqs_here, heads_here * head_size
    )
    normed = normed * head_gain.astype(jnp.float32)
    output = (jax.nn.silu(gating.astype(jnp.float32)) * normed).astype(jnp.bfloat16)
    return (output, new_memory)


def expert_hidden(chosen, gate_weight, up_weight):
    gate_value = jnp.dot(chosen, gate_weight, preferred_element_type=jnp.float32)
    up_value = jnp.dot(chosen, up_weight, preferred_element_type=jnp.float32)
    return (jax.nn.silu(gate_value) * up_value).astype(jnp.bfloat16)


def padded_experts(
    normed_mid, routes, route_weight, expert_gate, expert_up, expert_down, capacity, experts_all
):
    seq_dev, model_width = normed_mid.shape
    top_count = routes.shape[1]
    flat_ids = routes.reshape(-1)
    expert_ids = jnp.arange(experts_all, dtype=jnp.int32)
    onehot = (flat_ids[:, None] == expert_ids[None, :]).astype(jnp.int32)
    ranks = jnp.sum((jnp.cumsum(onehot, axis=0) - 1) * onehot, axis=1)
    slot_ids = flat_ids * capacity + ranks
    slot_range = jnp.arange(experts_all * capacity, dtype=jnp.int32)
    dispatch = (slot_range[:, None] == slot_ids[None, :]).astype(jnp.bfloat16)
    repeated = jnp.repeat(normed_mid, top_count, axis=0)
    outgoing = jnp.dot(dispatch, repeated, preferred_element_type=jnp.float32).astype(jnp.bfloat16)
    outgoing = outgoing.reshape(experts_all, capacity, model_width)
    arrived = lax.all_to_all(outgoing, "ep", split_axis=0, concat_axis=0, tiled=True)
    sources = arrived.shape[0]
    items = arrived.shape[1]
    hidden_e = expert_hidden(
        arrived.reshape(sources * items, model_width), expert_gate[0], expert_up[0]
    )
    partial_value = jnp.dot(hidden_e, expert_down[0], preferred_element_type=jnp.float32)
    summed = sent_and_summed(partial_value.astype(jnp.bfloat16), "tp", 1).astype(jnp.bfloat16)
    returned = lax.all_to_all(
        summed.reshape(sources, items, summed.shape[1]),
        "ep",
        split_axis=0,
        concat_axis=0,
        tiled=True,
    )
    flat_back = returned.reshape(experts_all * capacity, returned.shape[2])
    weighted = flat_back[slot_ids].astype(jnp.float32) * route_weight.reshape(-1)[:, None].astype(
        jnp.float32
    )
    return jnp.sum(weighted.reshape(seq_dev, top_count, weighted.shape[1]), axis=1)


def per_device(
    resid,
    norm_gain,
    w_query,
    w_key,
    w_value,
    w_gate,
    head_gain,
    w_output,
    state,
    positions,
    ffn_gain,
    w_mix,
    dense_gate,
    dense_up,
    dense_down,
    routes,
    route_weight,
    expert_gate,
    expert_up,
    expert_down,
):
    seq_dev = resid.shape[0]
    model_width = resid.shape[1]
    tp_count = lax.axis_size("tp")
    ep_count = lax.axis_size("ep")
    model_tp = model_width // tp_count
    tp_index = lax.axis_index("tp")
    normed_in = rms_norm(resid.astype(jnp.float32), norm_gain).astype(jnp.bfloat16)

    def project(weight):
        return jnp.dot(normed_in, weight, preferred_element_type=jnp.float32).astype(jnp.bfloat16)

    heads_here = state.shape[1]
    head_first = (tp_index * heads_here).astype(jnp.float32)
    retained, new_state = retain(
        project(w_query),
        project(w_key),
        project(w_value),
        project(w_gate),
        state,
        positions,
        head_first,
        head_gain,
    )
    partial_value = jnp.dot(retained, w_output, preferred_element_type=jnp.float32)
    attention = of_everyone(partial_value.astype(jnp.bfloat16), "tp").astype(jnp.float32)
    middle = resid.astype(jnp.float32) + attention
    normed_mid = rms_norm(middle, ffn_gain).astype(jnp.bfloat16)
    mixing = jax.nn.sigmoid(jnp.dot(normed_mid, w_mix[:, None], preferred_element_type=jnp.float32))

    def own_columns(matrix):
        return lax.dynamic_slice_in_dim(matrix, tp_index * model_tp, model_tp, 1)

    top_count = routes.shape[1]
    capacity = max(2, 2 * seq_dev * top_count // ep_count)
    dense_rows = gather_directly(own_columns(normed_mid), "ep", 0)
    moe_out = padded_experts(
        normed_mid, routes, route_weight, expert_gate, expert_up, expert_down, capacity, ep_count
    )
    gate_part = jnp.dot(dense_rows, dense_gate, preferred_element_type=jnp.float32)
    up_part = jnp.dot(dense_rows, dense_up, preferred_element_type=jnp.float32)
    gate_sum, up_sum = tuple(
        (
            part.astype(jnp.float32)
            for part in packed_total(
                (gate_part.astype(jnp.bfloat16), up_part.astype(jnp.bfloat16)), "tp"
            )
        )
    )
    dense_hidden = (jax.nn.silu(gate_sum) * up_sum).astype(jnp.bfloat16)
    dense_out = sent_and_summed(
        jnp.dot(dense_hidden, dense_down, preferred_element_type=jnp.float32).astype(jnp.bfloat16),
        "ep",
        0,
    )
    final = (own_columns(middle) + moe_out + mixing * dense_out).astype(jnp.bfloat16)
    return (final, new_state)


def solution(mesh):
    in_specs = (
        P("ep", None),
        P(),
        P(None, "tp"),
        P(None, "tp"),
        P(None, "tp"),
        P(None, "tp"),
        P("tp"),
        P("tp", None),
        P("ep", "tp", None, None),
        P("ep"),
        P(),
        P(),
        P("tp", "ep"),
        P("tp", "ep"),
        P("ep", "tp"),
        P("ep", None),
        P("ep", None),
        P("ep", None, "tp"),
        P("ep", None, "tp"),
        P("ep", "tp", None),
    )
    out_specs = (P("ep", "tp"), P("ep", "tp", None, None))
    return jax.shard_map(
        per_device, mesh=mesh, in_specs=in_specs, out_specs=out_specs, check_vma=False
    )
```

profile of v0, /device:TPU:24, one launch (start us, length us, event | category | flops | bytes accessed | tf_op | source)
XLA Modules:
  0.0 206.2 jit_solution(7254978397219586404)
XLA Ops:
  7.3 0.8 convert_element_type.126
  8.1 0.7 convert_element_type.121
  8.7 1.0 fusion.25
  9.8 0.7 convert_element_type.116
  10.5 1.4 fusion.18
  11.9 1.4 fusion.20
  13.3 0.1 fusion.44
  13.5 0.2 fusion.49
  13.6 2.0 fusion.66
  15.6 1.0 fusion.65
  16.6 0.2 multiply_reduce_fusion.2
  16.8 1.5 convolution_convert_fusion.2
  18.4 1.1 broadcast_in_dim.6
  19.5 5.4 %all-to-all-start = ((bf16[8,32,2048]{2,1,0:T(8,128)(2,1)}), bf16[8,32,2048]{2,1,0:T(8,128)(2,1)S(1)}, u32[]{:S(2)}, u32[]{:S(2)}) async-start(bf16[8,32,2048]{2,1,0:T(8,128)(2,1)} %broadcast_in_dim.6), calls=%async_computation | async-start | bytes 2097152 | tf_op jit(solution)/shard_map/all_to_all | solution.py:23
  24.9 0.1 copy.36
  25.0 13.7 %all-to-all-done = bf16[8,32,2048]{2,1,0:T(8,128)(2,1)S(1)} async-done(((bf16[8,32,2048]{2,1,0:T(8,128)(2,1)}), bf16[8,32,2048]{2,1,0:T(8,128)(2,1)S(1)}, u32[]{:S(2)}, u32[]{:S(2)}) %all-to-all-start) | async-done | bytes 1048608 | tf_op jit(solution)/shard_map/all_to_all | solution.py:23
  38.7 0.1 convert_reduce_fusion
  38.9 0.1 multiply_reduce_fusion
  39.0 0.7 copy-done.2
  39.8 0.1 multiply_convert_fusion.2
  39.9 0.9 broadcast_in_dim.8
  40.7 10.6 %all-to-all-start.4 = ((bf16[32,32,256]{2,1,0:T(8,128)(2,1)}), bf16[32,32,256]{2,1,0:T(8,128)(2,1)S(1)}, u32[]{:S(2)}, u32[]{:S(2)}) async-start(bf16[32,32,256]{2,1,0:T(8,128)(2,1)} %broadcast_in_dim.8), calls=%async_computation.4 | async-start | bytes 1048576 | tf_op jit(solution)/shard_map/all_to_all | solution.py:23
  51.4 0.1 copy.38
  51.4 0.7 mul.310
  52.1 0.1 reshape.383
  52.3 0.1 reduce_window_sum.11
  52.4 0.2 select_reduce_fusion
  52.6 0.5 copy-done.13
  53.1 0.1 broadcast_in_dim.7
  53.3 0.1 reshape.384
  53.4 0.3 convolution_convert_fusion.1
  53.7 1.0 reshape.385
  54.7 14.1 %all-to-all-done.4 = bf16[32,32,256]{2,1,0:T(8,128)(2,1)S(1)} async-done(((bf16[32,32,256]{2,1,0:T(8,128)(2,1)}), bf16[32,32,256]{2,1,0:T(8,128)(2,1)S(1)}, u32[]{:S(2)}, u32[]{:S(2)}) %all-to-all-start.4) | async-done | bytes 524320 | tf_op jit(solution)/shard_map/all_to_all | solution.py:23
  68.8 4.7 %all-to-all-start.1 = ((bf16[32,4,2048]{2,1,0:T(4,128)(2,1)}), bf16[32,4,2048]{2,1,0:T(4,128)(2,1)S(1)}, u32[]{:S(2)}, u32[]{:S(2)}) async-start(bf16[32,4,2048]{2,1,0:T(4,128)(2,1)} %reshape.385), calls=%async_computation.1 | async-start | bytes 1048576 | tf_op jit(solution)/shard_map/all_to_all | solution.py:116
  73.5 1.2 convolution_convert_fusion.4
  74.7 2.0 convolution_convert_fusion.5
  76.7 1.2 copy.40
  77.9 1.4 reshape.391
  79.3 0.2 copy.41
  79.5 0.7 reshape.392
  80.2 1.9 pad_maximum_fusion
  82.1 8.3 %all-to-all-done.1 = bf16[32,4,2048]{2,1,0:T(4,128)(2,1)S(1)} async-done(((bf16[32,4,2048]{2,1,0:T(4,128)(2,1)}), bf16[32,4,2048]{2,1,0:T(4,128)(2,1)S(1)}, u32[]{:S(2)}, u32[]{:S(2)}) %all-to-all-start.1) | async-done | bytes 524320 | tf_op jit(solution)/shard_map/all_to_all | solution.py:116
  90.5 0.1 reshape.386
  90.6 2.0 fusion.3
  92.6 2.5 %convolution_convert_fusion = bf16[128,2048]{1,0:T(8,128)(2,1)S(1)} fusion(bf16[1,512,2048]{2,1,0:T(8,128)(2,1)S(1)} %copy-done, bf16[128,2048]{1,0:T(8,128)(2,1)S(1)} %reshape.386, bf16[1,2048,512]{2,1,0:T(8,128)(2,1)} %param.38, f32[128,512]{1,0:T(8,128)S(1)} %fusion.3), kind=kOutput, calls=%fused_computation.1 | convolution fusion | flops 537526272 | bytes 5505024 | tf_op jit(solution)/shard_map/dot_general | solution.py:122
  95.1 0.8 copy.46
  95.9 6.1 %all-to-all-start.2 = ((bf16[8,128,256]{2,1,0:T(8,128)(2,1)}), bf16[8,128,256]{2,1,0:T(8,128)(2,1)}, u32[]{:S(2)}, u32[]{:S(2)}) async-start(bf16[8,128,256]{2,1,0:T(8,128)(2,1)} %bitcast.85), calls=%async_computation.2 | async-start | bytes 1048576 | tf_op jit(solution)/shard_map/all_to_all | solution.py:17
  102.0 47.7 %all-reduce.2.cloned.1.call-done = bf16[360448]{0:T(1024)(128)(2,1)} async-done(((bf16[360448]{0:T(1024)(128)(2,1)}), bf16[360448]{0:T(1024)(128)(2,1)}) %all-reduce.2.cloned.1.call-update) | async-done | bytes 720912 | tf_op jit(solution)/shard_map/psum | solution.py:44
  149.8 1.2 slice_convert_fusion.1
  150.9 1.7 reshape.401
  152.7 1.7 reshape.402
  154.4 1.1 reduce_sum.102
  155.5 0.6 reshape.388
  156.1 9.8 %all-to-all-start.3 = ((bf16[32,4,256]{2,1,0:T(4,128)(2,1)}), bf16[32,4,256]{2,1,0:T(4,128)(2,1)S(1)}, u32[]{:S(2)}, u32[]{:S(2)}) async-start(bf16[32,4,256]{2,1,0:T(4,128)(2,1)} %reshape.388), calls=%async_computation.3 | async-start | bytes 131072 | tf_op jit(solution)/shard_map/all_to_all | solution.py:124
  166.0 2.8 %convolution_convert_fusion.3 = bf16[1024,256]{1,0:T(8,128)(2,1)} fusion(bf16[176,256]{1,0:T(8,128)(2,1)S(1)} %copy-done.17, f32[1024,176]{1,0:T(8,128)} %reshape.402, f32[1024,176]{1,0:T(8,128)} %reshape.401), kind=kOutput, calls=%fused_computation.13 | convolution fusion | flops 93618176 | bytes 2056192 | tf_op jit(solution)/shard_map/dot_general | solution.py:210
  168.8 7.4 %all-to-all-done.3 = bf16[32,4,256]{2,1,0:T(4,128)(2,1)S(1)} async-done(((bf16[32,4,256]{2,1,0:T(4,128)(2,1)}), bf16[32,4,256]{2,1,0:T(4,128)(2,1)S(1)}, u32[]{:S(2)}, u32[]{:S(2)}) %all-to-all-start.3) | async-done | bytes 65568 | tf_op jit(solution)/shard_map/all_to_all | solution.py:124
  176.2 3.9 %all-to-all-start.5 = ((bf16[32,32,256]{2,1,0:T(8,128)(2,1)}), bf16[32,32,256]{2,1,0:T(8,128)(2,1)S(1)}, u32[]{:S(2)}, u32[]{:S(2)}) async-start(bf16[32,32,256]{2,1,0:T(8,128)(2,1)} %bitcast.18), calls=%async_computation.5 | async-start | bytes 1048576 | tf_op jit(solution)/shard_map/all_to_all | solution.py:17
  180.2 0.1 copy.39
  180.4 2.9 %multiply_add_fusion = f32[32,1,128,128]{3,2,1,0:T(8,128)} fusion(f32[32,1,128,128]{3,2,1,0:T(8,128)} %param.28, f32[32,128]{1,0:T(8,128)S(1)} %copy-done.9, f32[32,128]{1,0:T(8,128)S(1)} %maximum_multiply_fusion.1, f32[]{:T(128)S(6)} %sub.37), kind=kLoop, calls=%fused_computation.11 | loop fusion | flops 1572864 | bytes 4227076 | tf_op jit(solution)/shard_map/add | solution.py:83
  183.3 0.1 fusion.24
  183.5 0.7 gather_fusion
  184.2 0.1 multiply_reduce_fusion.1
  184.4 13.4 %all-to-all-done.5 = bf16[32,32,256]{2,1,0:T(8,128)(2,1)S(1)} async-done(((bf16[32,32,256]{2,1,0:T(8,128)(2,1)}), bf16[32,32,256]{2,1,0:T(8,128)(2,1)S(1)}, u32[]{:S(2)}, u32[]{:S(2)}) %all-to-all-start.5) | async-done | bytes 524320 | tf_op jit(solution)/shard_map/all_to_all | solution.py:17
  197.9 1.4 add_convert_fusion
  (54 shorter events, 0.5 us)
Async XLA Ops:
  7.2 85.5 %copy-start = (bf16[1,512,2048]{2,1,0:T(8,128)(2,1)S(1)}, bf16[1,512,2048]{2,1,0:T(8,128)(2,1)}, u32[]{:S(2)}) copy-start(bf16[1,512,2048]{2,1,0:T(8,128)(2,1)} %param.39) | copy-start | bytes 6291460
  7.2 8.4 %copy-start.1 = (bf16[32,2048]{1,0:T(8,128)(2,1)S(1)}, bf16[32,2048]{1,0:T(8,128)(2,1)}, u32[]{:S(2)}) copy-start(bf16[32,2048]{1,0:T(8,128)(2,1)} %param.20) | copy-start | bytes 393220
  7.2 8.4 %copy-start.5 = (bf16[2048,128]{1,0:T(8,128)(2,1)S(1)}, bf16[2048,128]{1,0:T(8,128)(2,1)}, u32[]{:S(2)}) copy-start(bf16[2048,128]{1,0:T(8,128)(2,1)} %param.24) | copy-start | bytes 1572868
  10.5 6.3 %copy-start.6 = (bf16[128,2048]{1,0:T(8,128)(2,1)S(1)}, bf16[128,2048]{1,0:T(8,128)(2,1)}, u32[]{:S(2)}) copy-start(bf16[128,2048]{1,0:T(8,128)(2,1)} %param.27) | copy-start | bytes 1572868
  13.4 4.9 %copy-start.7 = (f32[32,1,64]{2,0,1:T(8,128)}, f32[32,1,64]{2,0,1:T(8,128)S(1)}, u32[]{:S(2)}) copy-start(f32[32,1,64]{2,0,1:T(8,128)S(1)} %get-tuple-element.15) | copy-start | bytes 24580
  16.8 8.1 %copy-start.10 = (bf16[2048]{0:T(1024)(128)(2,1)S(1)}, bf16[2048]{0:T(1024)(128)(2,1)}, u32[]{:S(2)}) copy-start(bf16[2048]{0:T(1024)(128)(2,1)} %param.30) | copy-start | bytes 12292
  16.8 8.1 %copy-start.12 = (s32[32,2]{0,1:T(2,128)S(1)}, s32[32,2]{0,1:T(2,128)}, u32[]{:S(2)}) copy-start(s32[32,2]{0,1:T(2,128)} %param.35) | copy-start | bytes 772
  19.5 19.3 %all-to-all-start = ((bf16[8,32,2048]{2,1,0:T(8,128)(2,1)}), bf16[8,32,2048]{2,1,0:T(8,128)(2,1)S(1)}, u32[]{:S(2)}, u32[]{:S(2)}) async-start(bf16[8,32,2048]{2,1,0:T(8,128)(2,1)} %broadcast_in_dim.6), calls=%async_computation | async-start | bytes 2097152 | tf_op jit(solution)/shard_map/all_to_all | solution.py:23
  39.0 0.7 copy-start.2
  39.9 13.4 %copy-start.3 = (bf16[32,2048]{1,0:T(8,128)(2,1)}, bf16[32,2048]{1,0:T(8,128)(2,1)S(1)}, u32[]{:S(2)}) copy-start(bf16[32,2048]{1,0:T(8,128)(2,1)S(1)} %multiply_convert_fusion.2) | copy-start | bytes 393220
  40.7 28.1 %all-to-all-start.4 = ((bf16[32,32,256]{2,1,0:T(8,128)(2,1)}), bf16[32,32,256]{2,1,0:T(8,128)(2,1)S(1)}, u32[]{:S(2)}, u32[]{:S(2)}) async-start(bf16[32,32,256]{2,1,0:T(8,128)(2,1)} %broadcast_in_dim.8), calls=%async_computation.4 | async-start | bytes 1048576 | tf_op jit(solution)/shard_map/all_to_all | solution.py:23
  52.6 0.5 copy-start.13
  68.8 21.7 %all-to-all-start.1 = ((bf16[32,4,2048]{2,1,0:T(4,128)(2,1)}), bf16[32,4,2048]{2,1,0:T(4,128)(2,1)S(1)}, u32[]{:S(2)}, u32[]{:S(2)}) async-start(bf16[32,4,2048]{2,1,0:T(4,128)(2,1)} %reshape.385), calls=%async_computation.1 | async-start | bytes 1048576 | tf_op jit(solution)/shard_map/all_to_all | solution.py:116
  73.5 76.3 %all-reduce.2.cloned.1.call-start = ((), (), s32[]{:S(2)}) async-start(), calls=%async_computation.6 | async-start | bytes 1441792 | tf_op jit(solution)/shard_map/psum | solution.py:44
  95.9 58.4 %all-to-all-start.2 = ((bf16[8,128,256]{2,1,0:T(8,128)(2,1)}), bf16[8,128,256]{2,1,0:T(8,128)(2,1)}, u32[]{:S(2)}, u32[]{:S(2)}) async-start(bf16[8,128,256]{2,1,0:T(8,128)(2,1)} %bitcast.85), calls=%async_computation.2 | async-start | bytes 1048576 | tf_op jit(solution)/shard_map/all_to_all | solution.py:17
  152.7 13.3 %copy-start.17 = (bf16[176,256]{1,0:T(8,128)(2,1)S(1)}, bf16[176,256]{1,0:T(8,128)(2,1)}, u32[]{:S(2)}) copy-start(bf16[176,256]{1,0:T(8,128)(2,1)} %param.34) | copy-start | bytes 270340
  156.1 20.1 %all-to-all-start.3 = ((bf16[32,4,256]{2,1,0:T(4,128)(2,1)}), bf16[32,4,256]{2,1,0:T(4,128)(2,1)S(1)}, u32[]{:S(2)}, u32[]{:S(2)}) async-start(bf16[32,4,256]{2,1,0:T(4,128)(2,1)} %reshape.388), calls=%async_computation.3 | async-start | bytes 131072 | tf_op jit(solution)/shard_map/all_to_all | solution.py:124
  166.0 14.1 %copy-start.14 = (s32[64]{0:T(128)S(1)}, s32[64]{0:T(128)}, u32[]{:S(2)}) copy-start(s32[64]{0:T(128)} %copy-done.13) | copy-start | bytes 772
  166.0 14.1 %copy-start.16 = (s32[64,1]{0,1:T(1,128)S(1)}, s32[64,1]{0,1:T(1,128)}, u32[]{:S(2)}) copy-start(s32[64,1]{0,1:T(1,128)} %mul.310) | copy-start | bytes 772
  166.0 14.1 %copy-start.11 = (bf16[2048]{0:T(1024)(128)(2,1)S(1)}, bf16[2048]{0:T(1024)(128)(2,1)}, u32[]{:S(2)}) copy-start(bf16[2048]{0:T(1024)(128)(2,1)} %param.31) | copy-start | bytes 12292
  166.0 14.2 %copy-start.15 = (bf16[32,2]{0,1:T(2,128)(2,1)S(1)}, bf16[32,2]{0,1:T(2,128)(2,1)}, u32[]{:S(2)}) copy-start(bf16[32,2]{0,1:T(2,128)(2,1)} %param.36) | copy-start | bytes 388
  166.0 14.3 %copy-start.8 = (f32[32,1,64]{2,0,1:T(8,128)S(1)}, f32[32,1,64]{2,0,1:T(8,128)}, u32[]{:S(2)}) copy-start(f32[32,1,64]{2,0,1:T(8,128)} %copy-done.7) | copy-start | bytes 24580
  166.0 14.3 %copy-start.9 = (f32[32,128]{1,0:T(8,128)S(1)}, f32[32,128]{1,0:T(8,128)}, u32[]{:S(2)}) copy-start(f32[32,128]{1,0:T(8,128)} %get-tuple-element.16) | copy-start | bytes 49156
  176.2 21.6 %all-to-all-start.5 = ((bf16[32,32,256]{2,1,0:T(8,128)(2,1)}), bf16[32,32,256]{2,1,0:T(8,128)(2,1)S(1)}, u32[]{:S(2)}, u32[]{:S(2)}) async-start(bf16[32,32,256]{2,1,0:T(8,128)(2,1)} %bitcast.18), calls=%async_computation.5 | async-start | bytes 1048576 | tf_op jit(solution)/shard_map/all_to_all | solution.py:17
  180.4 2.9 %copy-start.4 = (bf16[32,2048]{1,0:T(8,128)(2,1)S(1)}, bf16[32,2048]{1,0:T(8,128)(2,1)}, u32[]{:S(2)}) copy-start(bf16[32,2048]{1,0:T(8,128)(2,1)} %copy-done.3) | copy-start | bytes 393220
Sparse Core Ops, SparseCore 0:
  82.2 67.4 all-reduce.1
where the time goes:
time: 207 us; the launch traced here: 206 us
  waiting for transfers between devices  105 us (51%)
  starting transfers between devices  40.5 us (20%)
  matrix products  18.1 us (9%)
  local copies, waits for them, and re-layouts  14.9 us (7%)
  between operations  14.5 us (7%)
  other arithmetic  13.4 us (6%)
    psum x1, waiting for transfers between devices, packed_total(): running = lax.psum(flat, axis)  47.7 us
    all_to_all x2, waiting for transfers between devices, copy_for_each(): return lax.all_to_all(copies, axis, split_axis=0, concat_axis=0, tiled=True)  27.9 us
    all_to_all x2, starting transfers between devices, copy_for_each(): return lax.all_to_all(copies, axis, split_axis=0, concat_axis=0, tiled=True)  16 us
    all_to_all x2, waiting for transfers between devices, sent_and_summed(): lax.all_to_all(tiles, axis, split_axis=0, concat_axis=0, tiled=True)  13.4 us
    all_to_all x2, starting transfers between devices, sent_and_summed(): lax.all_to_all(tiles, axis, split_axis=0, concat_axis=0, tiled=True)  9.98 us
    all_to_all x1, starting transfers between devices, padded_experts(): lax.all_to_all(summed.reshape(sources, items, summed.shape[1]), 'ep', spl...  9.82 us
    all_to_all x1, waiting for transfers between devices, padded_experts(): lax.all_to_all(outgoing, 'ep', split_axis=0, concat_axis=0, tiled=True)  8.34 us
    all_to_all x1, waiting for transfers between devices, padded_experts(): lax.all_to_all(summed.reshape(sources, items, summed.shape[1]), 'ep', spl...  7.39 us
  transfers between devices with their start and end apart: 7, of which 6 were waited for; matrix products, arithmetic and copies ran while one was open for 14% of the time, Pallas kernels for 0%

commit v1 on v0

v1 whole, which is shorter than its diff:
```python
import jax
import jax.numpy as jnp
from jax import lax
from jax.sharding import Mesh, PartitionSpec as P

EPSILON = 1e-06
THETA = 10000.0
EP = ("z", "x")
TP = ("y", "c")
BF = jnp.bfloat16
F32 = jnp.float32


def exchange(value, axis):
    return lax.all_to_all(value, axis, split_axis=0, concat_axis=0, tiled=True)


def swap_cores(value):
    return lax.ppermute(value, "c", [(0, 1), (1, 0)])


def dot(a, b):
    return jnp.dot(a, b, preferred_element_type=F32)


def dot_nt(a, b):
    return lax.dot_general(a, b, (((1,), (1,)), ((), ())), preferred_element_type=F32)


def dot_tn(a, b):
    return lax.dot_general(a, b, (((0,), (0,)), ((), ())), preferred_element_type=F32)


def rms_norm(inputs, scaling):
    square = jnp.mean(inputs * inputs, axis=-1, keepdims=True)
    return inputs * lax.rsqrt(square + EPSILON) * scaling.astype(F32)


def rotate(inputs, places):
    halfway = inputs.shape[-1] // 2
    inverse = THETA ** (-jnp.arange(halfway, dtype=F32) / halfway)
    angles = places.astype(F32)[:, None] * inverse[None, :]
    cosine = jnp.cos(angles)[:, None, :]
    sine_of = jnp.sin(angles)[:, None, :]
    former = inputs[..., :halfway]
    latter = inputs[..., halfway:]
    return jnp.concatenate(
        [former * cosine - latter * sine_of, former * sine_of + latter * cosine], axis=-1
    )


def retain(queries, keys_in, values_in, gating, memory, places, head_first, head_gain):
    seqs_here = queries.shape[0]
    heads_here = memory.shape[1]
    head_size = memory.shape[2]
    head_shape = (seqs_here, heads_here, head_size)
    query_rot = rotate(queries.astype(F32).reshape(head_shape), places)
    key_rot = rotate(keys_in.astype(F32).reshape(head_shape), places) * head_size ** (-0.5)
    value_heads = values_in.astype(F32).reshape(head_shape)
    head_index = head_first + jnp.arange(heads_here, dtype=F32)
    decays = 1.0 - jnp.exp2(-1.0 - 1.5 * head_index)
    within = jnp.sum(query_rot * key_rot, axis=-1, keepdims=True) * value_heads
    carried = jnp.einsum("shd,shde->she", query_rot, memory) * decays[None, :, None]
    mixture = within + carried
    new_memory = (
        decays[None, :, None, None] * memory + key_rot[:, :, :, None] * value_heads[:, :, None, :]
    )
    centre = jnp.mean(mixture, axis=-1, keepdims=True)
    spread = jnp.mean(jnp.square(mixture - centre), axis=-1, keepdims=True)
    normed = ((mixture - centre) * lax.rsqrt(spread + EPSILON)).reshape(
        seqs_here, heads_here * head_size
    )
    normed = normed * head_gain.astype(F32)
    output = (jax.nn.silu(gating.astype(F32)) * normed).astype(BF)
    return (output, new_memory)


def row_places(routes, experts):
    ids = jnp.arange(experts, dtype=jnp.int32)
    named = jnp.any(routes[:, :, None] == ids[None, None, :], axis=1).astype(jnp.int32)
    before = jnp.cumsum(named, axis=0) - named
    total = jnp.sum(named, axis=0, keepdims=True)
    earlier = jnp.arange(routes.shape[0], dtype=jnp.int32)[:, None]
    return jnp.where(named == 1, before, total + earlier - before)


def per_device(
    resid, norm_gain, w_query, w_key, w_value, w_gate, head_gain, w_output, state, positions,
    ffn_gain, w_mix, dense_gate, dense_up, dense_down, routes, route_weight,
    expert_gate, expert_up, expert_down,
):
    seqs, width = resid.shape
    n_y, n_c = lax.axis_size("y"), lax.axis_size("c")
    n_tp = n_y * n_c
    n_ep = lax.axis_size("z") * lax.axis_size("x")
    cols = width // n_tp
    core = lax.axis_index("c")
    tp = lax.axis_index("y") * n_c + core
    slots = max(2, 2 * seqs * routes.shape[1] // n_ep)
    hid = dense_gate.shape[1]

    own_w = jnp.concatenate([dense_gate.T, dense_up.T], axis=0)
    pair_w = jnp.concatenate([own_w, swap_cores(own_w)], axis=1)

    normed_in = rms_norm(resid.astype(F32), norm_gain).astype(BF)

    def project(weight):
        return dot(normed_in, weight).astype(BF)

    heads_here = state.shape[1]
    retained, new_state = retain(
        project(w_query), project(w_key), project(w_value), project(w_gate),
        state, positions, (tp * heads_here).astype(F32), head_gain,
    )
    partial = dot(retained, w_output).astype(BF)
    partial = jnp.moveaxis(partial.reshape(seqs, n_tp, cols), 1, 0)
    arrived = exchange(partial, TP)

    def own_columns(matrix, block):
        return lax.dynamic_slice_in_dim(matrix, block * cols, cols, matrix.ndim - 1)

    middle = own_columns(resid, tp).astype(F32) + jnp.sum(arrived.astype(F32), axis=0)
    middle_cut = middle.astype(BF)

    place = row_places(routes, n_ep)
    sorting = (place.T[:, None, :] == jnp.arange(seqs, dtype=jnp.int32)[None, :, None]).astype(BF)
    sorting = sorting.reshape(n_ep * seqs, seqs)
    outgoing = dot(sorting, middle_cut).astype(BF).reshape(n_ep, seqs, cols)
    rows = exchange(outgoing, EP)

    chosen = rows[:, :slots].reshape(n_ep * slots, cols)
    chosen_other = swap_cores(chosen)
    flat = rows.reshape(n_ep * seqs, cols)
    half = n_ep * seqs // n_c
    kept = lax.dynamic_slice_in_dim(flat, core * half, half, 0)
    gained = swap_cores(lax.dynamic_slice_in_dim(flat, (1 - core) * half, half, 0))
    both = jnp.concatenate([kept, gained], axis=1).astype(F32)
    gains = jnp.concatenate([own_columns(ffn_gain, tp), own_columns(ffn_gain, tp ^ 1)])
    mixers = jnp.concatenate([own_columns(w_mix, tp), own_columns(w_mix, tp ^ 1)])
    scaled = (both * gains.astype(F32)).astype(BF)
    weights = jnp.concatenate([pair_w, mixers[None, :], jnp.zeros((7, n_c * cols), BF)], axis=0)
    sums = dot_nt(weights, scaled)
    squares = dot_nt(jnp.ones((8, n_c * cols), BF), (both * both).astype(BF))
    lower = jnp.concatenate([sums[2 * hid : 2 * hid + 1], squares[:7]], axis=0)
    sums = jnp.concatenate([sums[: 2 * hid], lower], axis=0).astype(BF)
    part = half // n_y
    sums = jnp.moveaxis(sums.reshape(2 * hid + 8, n_y, part), 1, 0)
    ordered = jnp.where(core == 0, jnp.concatenate([chosen, chosen_other], axis=1),
                        jnp.concatenate([chosen_other, chosen], axis=1))
    n_slots = n_ep * slots
    pieces = jnp.moveaxis(ordered.reshape(n_slots, n_c * cols // part, part), 1, 0)
    pieces = pieces.reshape(1, -1, part)
    sent = jnp.concatenate([sums, jnp.broadcast_to(pieces, (n_y, *pieces.shape[1:]))], axis=1)
    got = exchange(sent, "y")

    sums = jnp.sum(got[:, : 2 * hid + 8].astype(F32), axis=0)
    scale = lax.rsqrt(sums[2 * hid + 1 : 2 * hid + 2] / width + EPSILON)
    mixing = jax.nn.sigmoid(sums[2 * hid : 2 * hid + 1] * scale)
    dense_hidden = jax.nn.silu(sums[:hid] * scale) * (sums[hid : 2 * hid] * scale) * mixing
    dense_hidden = dense_hidden.astype(BF)
    hidden_pair = swap_cores(dense_hidden)

    pieces = got[:, 2 * hid + 8 :].reshape(n_y * n_c * cols // part, n_slots, part)
    chosen = jnp.moveaxis(pieces, 0, 1).reshape(n_slots, width).astype(F32)
    chosen = rms_norm(chosen, ffn_gain).astype(BF)
    hidden = jax.nn.silu(dot(chosen, expert_gate[0])) * dot(chosen, expert_up[0])
    down = dot(hidden.astype(BF), expert_down[0]).astype(BF)
    down = jnp.moveaxis(down.reshape(n_slots, n_y, n_c, cols), 2, 0)
    down_kept = lax.dynamic_index_in_dim(down, core, 0, False)
    down_got = swap_cores(lax.dynamic_index_in_dim(down, 1 - core, 0, False))
    down = (down_kept.astype(F32) + down_got.astype(F32)).astype(BF)
    down = jnp.moveaxis(down.reshape(n_slots, n_y, cols // part, part), 0, 2)
    down = down.reshape(n_y, cols // part * n_slots, part)
    hiddens = jnp.where(core == 0, jnp.concatenate([dense_hidden, hidden_pair], axis=0),
                        jnp.concatenate([hidden_pair, dense_hidden], axis=0))
    sent = jnp.concatenate([down, jnp.broadcast_to(hiddens[None], (n_y, *hiddens.shape))], axis=1)
    got = exchange(sent, "y")

    at = cols // part * n_slots
    result = jnp.sum(got[:, :at].astype(F32), axis=0).astype(BF)
    result = result.reshape(cols // part, n_ep, slots, part)
    hiddens = got[:, at:].reshape(n_y, n_c, hid, part)
    hiddens = jnp.moveaxis(hiddens, 2, 0)
    hiddens = jnp.moveaxis(hiddens, 2, 1).reshape(hid, n_ep * seqs)
    dense_back = dot_tn(hiddens, dense_down).astype(BF).reshape(n_ep, seqs, cols)
    back = jnp.concatenate(
        [dense_back[:, :, i * part : (i + 1) * part] for i in range(cols // part)]
        + [result[i] for i in range(cols // part)], axis=1,
    )
    back = exchange(back, EP)

    ids = jnp.arange(n_ep, dtype=jnp.int32)
    slot_ids = jnp.arange(slots, dtype=jnp.int32)
    weight_of = jnp.sum(
        jnp.where(routes[:, :, None] == ids, route_weight.astype(F32)[:, :, None], 0.0), axis=1
    )
    weighing = jnp.where(place[:, :, None] == slot_ids, weight_of[:, :, None], 0.0).astype(BF)
    weighing = weighing.reshape(seqs, n_slots)
    total = []
    for i in range(cols // part):
        dense_rows = back[:, i * seqs : (i + 1) * seqs].reshape(n_ep * seqs, part)
        first = cols // part * seqs + i * slots
        expert_rows = back[:, first : first + slots].reshape(n_slots, part)
        total.append(dot_tn(sorting, dense_rows) + dot(weighing, expert_rows))
    final = (middle + jnp.concatenate(total, axis=1)).astype(BF)
    return (final, new_state)


def solution(mesh):
    inner = Mesh(mesh.devices.reshape(8, 4, 4, 2), ("z", "x", "y", "c"))
    in_specs = (
        P(EP, None), P(), P(None, TP), P(None, TP), P(None, TP), P(None, TP), P(TP), P(TP, None),
        P(EP, TP, None, None), P(EP), P(), P(), P(TP, EP), P(TP, EP), P(EP, TP),
        P(EP, None), P(EP, None), P(EP, None, TP), P(EP, None, TP), P(EP, TP, None),
    )
    out_specs = (P(EP, TP), P(EP, TP, None, None))
    return jax.shard_map(
        per_device, mesh=inner, in_specs=in_specs, out_specs=out_specs, check_vma=False
    )
```

time: 207 us -> 130 us (0.63)
  waiting for transfers between devices: 105 us -> 48.7 us
  blocking collectives: 0 us -> 13.8 us
  between operations: 14.5 us -> 1.51 us
  starting transfers between devices: 40.5 us -> 27.6 us
  local copies, waits for them, and re-layouts: 14.9 us -> 8.09 us
  other arithmetic: 13.4 us -> 11.3 us
    psum x1 -> x0, waiting for transfers between devices: 47.7 us -> none  [packed_total(): running = lax.psum(flat, axis)]
    all_to_all x6 -> x4, starting transfers between devices: 40.5 us -> 26.2 us  [exchange(): return lax.all_to_all(value, axis, split_axis=0, concat_axis=0, tiled=True)]
    all_to_all x0 -> x1, blocking collectives: none -> 13.8 us  [exchange(): return lax.all_to_all(value, axis, split_axis=0, concat_axis=0, tiled=True)]
    all_to_all x6 -> x4, waiting for transfers between devices: 57 us -> 46.9 us  [exchange(): return lax.all_to_all(value, axis, split_axis=0, concat_axis=0, tiled=True)]
    convert_element_type x6 -> x1, local copies, waits for them, and re-layouts: 4.95 us -> 0.28 us  [per_device(): chosen = rms_norm(chosen, ffn_gain).astype(BF)]
    reshape x9 -> x4, local copies, waits for them, and re-layouts: 4.95 us -> 1.31 us  [the longest x1 0.66 us: per_device(): partial = jnp.moveaxis(partial.reshape(seqs, n_tp, cols), 1, 0)]
    convert_element_type x8 -> x9, other arithmetic: 4.97 us -> 3.08 us  [the longest x1 0.84 us: rms_norm(): return inputs * lax.rsqrt(square + EPSILON) * scaling.astype(F32)]
    dot_general x11 -> x14, matrix products: 16.1 us -> 15 us  [the longest x9 11.3 us: dot(): return jnp.dot(a, b, preferred_element_type=F32)]
  transfers between devices with their start and end apart: 7 -> 9, of which waited for: 6 -> 6; matrix products, arithmetic and copies ran while one was open for 14% -> 7% of each run, Pallas kernels for 0% -> 0%
where the time goes in v1:
time: 130 us; the launch traced here: 128 us
  waiting for transfers between devices  48.7 us (37%)
  starting transfers between devices  27.6 us (21%)
  matrix products  17 us (13%)
  blocking collectives  13.8 us (11%)
  other arithmetic  11.3 us (9%)
  local copies, waits for them, and re-layouts  8.09 us (6%)
  between operations  1.51 us (1%)
    all_to_all x4, waiting for transfers between devices, exchange(): return lax.all_to_all(value, axis, split_axis=0, concat_axis=0, tiled=True)  46.9 us
    all_to_all x4, starting transfers between devices, exchange(): return lax.all_to_all(value, axis, split_axis=0, concat_axis=0, tiled=True)  26.2 us
    all_to_all x1, blocking collectives, exchange(): return lax.all_to_all(value, axis, split_axis=0, concat_axis=0, tiled=True)  13.8 us
    dot_general x9, matrix products, dot(): return jnp.dot(a, b, preferred_element_type=F32)  11.3 us
    add x1, other arithmetic, retain(): decays[None, :, None, None] * memory  2.9 us
    dot_general x2, matrix products, dot_nt(): lax.dot_general(a, b, (((1,), (1,)), ((), ())), preferred_element_type=F32)  2.74 us
  transfers between devices with their start and end apart: 9, of which 6 were waited for; matrix products, arithmetic and copies ran while one was open for 7% of the time, Pallas kernels for 0%

profile of v1, /device:TPU:24, one launch (start us, length us, event | category | flops | bytes accessed | tf_op | source)
XLA Modules:
  0.0 128.0 jit_solution(16294772168796041397)
XLA Ops:
  0.7 0.8 convert_element_type.146
  1.5 1.0 fusion.45
  2.6 0.7 convert_element_type.151
  3.2 1.4 %fusion.20 = f32[32,1,128]{2,0,1:T(8,128)S(1)} fusion(bf16[2048,128]{1,0:T(8,128)(2,1)} %param.22, bf16[32,2048]{1,0:T(8,128)(2,1)} %param.20, f32[2048]{0:T(1024)S(1)} %convert_element_type.146, f32[32]{0:T(128)S(1)} %add_rsqrt_fusion.2), kind=kOutput, calls=%fused_computation.31 | convolution fusion | flops 17047552 | bytes 680064 | tf_op jit(solution)/shard_map/dot_general | solution.py:23
  4.7 1.4 %fusion.22 = f32[32,1,128]{2,0,1:T(8,128)S(1)} fusion(bf16[2048,128]{1,0:T(8,128)(2,1)} %param.23, bf16[32,2048]{1,0:T(8,128)(2,1)} %param.20, f32[2048]{0:T(1024)S(1)} %convert_element_type.146, f32[32]{0:T(128)S(1)} %add_rsqrt_fusion.2), kind=kOutput, calls=%fused_computation.33 | convolution fusion | flops 17047552 | bytes 680064 | tf_op jit(solution)/shard_map/dot_general | solution.py:23
  6.1 0.7 convert_element_type.156
  6.8 0.1 fusion.84
  6.9 0.6 copy-done.10
  7.5 0.2 fusion.89
  7.7 2.0 %fusion.122 = f32[32,1,128]{2,1,0:T(1,128)S(1)} fusion(f32[32,128,1]{1,2,0:T(1,128)S(1)} %bitcast.150, f32[32,1,128,128]{3,2,1,0:T(8,128)} %param.28), kind=kOutput, calls=%fused_computation.181 | convolution fusion | flops 1048576 | bytes 2129920 | tf_op jit(solution)/shard_map/shd,shde->she/dot_general | solution.py:63
  9.7 1.0 fusion.116
  10.7 0.2 multiply_reduce_fusion
  10.9 1.5 %convolution_convert_fusion.1 = bf16[32,2048]{1,0:T(8,128)(2,1)S(1)} fusion(bf16[128,2048]{1,0:T(8,128)(2,1)S(1)} %copy-done.5, bf16[2048,128]{1,0:T(8,128)(2,1)} %param.25, f32[32,128]{1,0:T(8,128)S(1)} %get-tuple-element.3, f32[128]{0:T(128)S(1)} %convert_element_type.156, f32[32]{0:T(128)S(1)} %add_rsqrt_fusion.1, f32[32]{0:T(128)S(1)} %broadcast_multiply_fusion, ...), kind=kOutput, calls=%fused_computation.1 | convolution fusion | flops 33927168 | bytes 1336192 | tf_op jit(solution)/shard_map/dot_general | solution.py:23
  12.4 0.7 copy.128
  13.1 5.2 %all-to-all-start = ((bf16[8,32,256]{2,1,0:T(8,128)(2,1)}), bf16[8,32,256]{2,1,0:T(8,128)(2,1)S(1)}, u32[]{:S(2)}, u32[]{:S(2)}) async-start(bf16[8,32,256]{2,1,0:T(8,128)(2,1)} %bitcast.126), calls=%async_computation | async-start | bytes 262144 | tf_op jit(solution)/shard_map/all_to_all | solution.py:15
  18.6 0.2 eq.81
  18.8 0.3 copy-done.22
  19.0 0.2 eq.84
  19.3 3.0 %all-to-all-done = bf16[8,32,256]{2,1,0:T(8,128)(2,1)S(1)} async-done(((bf16[8,32,256]{2,1,0:T(8,128)(2,1)}), bf16[8,32,256]{2,1,0:T(8,128)(2,1)S(1)}, u32[]{:S(2)}, u32[]{:S(2)}) %all-to-all-start) | async-done | bytes 131104 | tf_op jit(solution)/shard_map/all_to_all | solution.py:15
  22.4 1.1 convolution_convert_fusion.3
  23.6 10.8 %all-to-all-start.1 = ((bf16[32,32,256]{2,1,0:T(8,128)(2,1)}), bf16[32,32,256]{2,1,0:T(8,128)(2,1)S(1)}, u32[]{:S(2)}, u32[]{:S(2)}) async-start(bf16[32,32,256]{2,1,0:T(8,128)(2,1)} %bitcast.15), calls=%async_computation.1 | async-start | bytes 1048576 | tf_op jit(solution)/shard_map/all_to_all | solution.py:15
  34.4 0.1 collective-permute-start
  34.5 0.8 fusion.120
  35.4 16.5 %all-to-all-done.1 = bf16[32,32,256]{2,1,0:T(8,128)(2,1)S(1)} async-done(((bf16[32,32,256]{2,1,0:T(8,128)(2,1)}), bf16[32,32,256]{2,1,0:T(8,128)(2,1)S(1)}, u32[]{:S(2)}, u32[]{:S(2)}) %all-to-all-start.1) | async-done | bytes 524320 | tf_op jit(solution)/shard_map/all_to_all | solution.py:15
  51.9 0.1 collective-permute-start.1
  52.1 0.6 broadcast_in_dim.28
  52.7 0.7 pad.30.clone
  53.4 0.6 collective-permute-start.2
  54.0 0.9 collective-permute-done.2
  54.8 0.1 copy.93
  55.0 0.1 copy.94
  55.1 0.2 fusion.57
  55.4 1.2 fusion.29
  56.6 0.6 fusion.92
  57.2 1.5 %fusion.31 = bf16[360,512]{1,0:T(8,128)(2,1)S(1)} fusion(f32[512]{0:T(512)S(1)} %maximum_convert_fusion, bf16[1,512]{1,0:T(2,128)(2,1)} %broadcast_in_dim.28, bf16[352,256]{1,0:T(8,128)(2,1)} %collective-permute-done, bf16[176,256]{1,0:T(8,128)(2,1)} %bitcast.145, bf16[176,256]{1,0:T(8,128)(2,1)} %bitcast.147, bf16[512,256]{1,0:T(8,128)(2,1)} %collective-permute-done.1, ...), kind=kOutput, calls=%fused_computation.46 | convolution fusion | flops 192159744 | bytes 1257168 | tf_op jit(solution)/shard_map/dot_general | solution.py:27
  58.7 0.3 concatenate.111
  59.2 1.0 pad_maximum_fusion
  60.2 5.5 %all-to-all-start.2 = ((bf16[4,872,128]{2,1,0:T(8,128)(2,1)}), bf16[4,872,128]{2,1,0:T(8,128)(2,1)S(1)}, u32[]{:S(2)}, u32[]{:S(2)}) async-start(bf16[4,872,128]{2,1,0:T(8,128)(2,1)} %pad_maximum_fusion), calls=%async_computation.2 | async-start | bytes 1785856 | tf_op jit(solution)/shard_map/all_to_all | solution.py:15
  65.7 12.2 %all-to-all-done.2 = bf16[4,872,128]{2,1,0:T(8,128)(2,1)S(1)} async-done(((bf16[4,872,128]{2,1,0:T(8,128)(2,1)}), bf16[4,872,128]{2,1,0:T(8,128)(2,1)S(1)}, u32[]{:S(2)}, u32[]{:S(2)}) %all-to-all-start.2) | async-done | bytes 892960 | tf_op jit(solution)/shard_map/all_to_all | solution.py:15
  77.9 0.6 fusion.109
  78.5 0.2 fusion.25
  78.7 0.2 fusion.28
  79.0 0.3 copy.97
  79.3 2.1 %fusion.3 = f32[128,512]{1,0:T(8,128)S(1)} fusion(bf16[128,2048]{0,1:T(8,128)(2,1)S(1)} %bitcast.130, bf16[1,2048,512]{2,1,0:T(8,128)(2,1)} %param.37), kind=kOutput, calls=%fused_computation.5 | convolution fusion | flops 268435456 | bytes 2883584 | tf_op jit(solution)/shard_map/dot_general | solution.py:23
  81.3 2.4 %convolution_convert_fusion = bf16[128,2048]{1,0:T(8,128)(2,1)S(1)} fusion(bf16[1,512,2048]{2,1,0:T(8,128)(2,1)S(1)} %copy-done, bf16[128,2048]{0,1:T(8,128)(2,1)S(1)} %bitcast.131, bf16[1,2048,512]{2,1,0:T(8,128)(2,1)} %param.38, f32[128,512]{1,0:T(8,128)S(1)} %fusion.3), kind=kOutput, calls=%fused_computation | convolution fusion | flops 537526272 | bytes 5505024 | tf_op jit(solution)/shard_map/dot_general | solution.py:23
  83.8 0.4 reshape.435
  84.2 1.1 constant_dynamic-slice_fusion.1
  85.6 0.6 collective-permute-start.4
  86.1 0.9 collective-permute-done.4
  87.1 0.1 copy_bitcast_fusion
  87.4 13.8 %all_to_all.25 = bf16[4,608,128]{2,1,0:T(8,128)(2,1)S(1)} all-to-all(bf16[4,608,128]{2,1,0:T(8,128)(2,1)S(1)} %pad_maximum_fusion.1), channel_id=1, replica_groups=mesh['z'=8,'x'=4,'y'=4,'c'=2] {'y'}, dimensions={0} | all-to-all | bytes 1245184 | tf_op jit(solution)/shard_map/all_to_all | solution.py:15
  101.2 0.2 copy.101
  101.4 0.2 reshape.439
  101.8 0.4 convolution_convert_fusion.2
  102.2 0.9 pad_maximum_fusion.2
  103.1 4.7 %all-to-all-start.4 = ((bf16[32,72,128]{2,1,0:T(8,128)(2,1)}), bf16[32,72,128]{2,1,0:T(8,128)(2,1)S(1)}, u32[]{:S(2)}, u32[]{:S(2)}) async-start(bf16[32,72,128]{2,1,0:T(8,128)(2,1)} %pad_maximum_fusion.2), calls=%async_computation.4 | async-start | bytes 1179648 | tf_op jit(solution)/shard_map/all_to_all | solution.py:15
  108.0 0.2 iota_compare_fusion
  108.3 2.9 %multiply_add_fusion = f32[32,1,128,128]{3,2,1,0:T(8,128)} fusion(f32[32,1,128,128]{3,2,1,0:T(8,128)} %param.28, f32[32,128]{1,0:T(8,128)S(1)} %copy-done.19, f32[32,128]{1,0:T(8,128)S(1)} %maximum_multiply_fusion.1, f32[]{:T(128)S(6)} %sub.62), kind=kLoop, calls=%fused_computation.9 | loop fusion | flops 1572864 | bytes 4227076 | tf_op jit(solution)/shard_map/add | solution.py:66
  111.2 15.2 %all-to-all-done.4 = bf16[32,72,128]{2,1,0:T(8,128)(2,1)S(1)} async-done(((bf16[32,72,128]{2,1,0:T(8,128)(2,1)}), bf16[32,72,128]{2,1,0:T(8,128)(2,1)S(1)}, u32[]{:S(2)}, u32[]{:S(2)}) %all-to-all-start.4) | async-done | bytes 589856 | tf_op jit(solution)/shard_map/all_to_all | solution.py:15
  126.4 0.2 convolution_bitcast_fusion
  126.6 0.2 convolution_bitcast_fusion.1
  126.8 0.3 fusion.16
  127.1 0.3 fusion.15
  127.4 0.6 fusion.64
  (102 shorter events, 1.5 us)
Async XLA Ops:
  0.6 80.7 %copy-start = (bf16[1,512,2048]{2,1,0:T(8,128)(2,1)S(1)}, bf16[1,512,2048]{2,1,0:T(8,128)(2,1)}, u32[]{:S(2)}) copy-start(bf16[1,512,2048]{2,1,0:T(8,128)(2,1)} %param.39) | copy-start | bytes 6291460
  0.6 9.1 %copy-start.1 = (bf16[32,2048]{1,0:T(8,128)(2,1)S(1)}, bf16[32,2048]{1,0:T(8,128)(2,1)}, u32[]{:S(2)}) copy-start(bf16[32,2048]{1,0:T(8,128)(2,1)} %param.20) | copy-start | bytes 393220
  0.7 9.0 %copy-start.4 = (bf16[2048,128]{1,0:T(8,128)(2,1)S(1)}, bf16[2048,128]{1,0:T(8,128)(2,1)}, u32[]{:S(2)}) copy-start(bf16[2048,128]{1,0:T(8,128)(2,1)} %param.24) | copy-start | bytes 1572868
  3.2 7.7 %copy-start.5 = (bf16[128,2048]{1,0:T(8,128)(2,1)S(1)}, bf16[128,2048]{1,0:T(8,128)(2,1)}, u32[]{:S(2)}) copy-start(bf16[128,2048]{1,0:T(8,128)(2,1)} %param.27) | copy-start | bytes 1572868
  6.9 0.6 copy-start.10
  6.9 0.8 copy-start.12
  7.7 10.6 %copy-start.24 = (s32[32,2]{0,1:T(2,128)S(1)}, s32[32,2]{0,1:T(2,128)}, u32[]{:S(2)}) copy-start(s32[32,2]{0,1:T(2,128)} %param.35) | copy-start | bytes 772
  12.4 21.9 %copy-start.16 = (bf16[256,176]{0,1:T(8,128)(2,1)S(1)}, bf16[256,176]{0,1:T(8,128)(2,1)}, u32[]{:S(2)}) copy-start(bf16[256,176]{0,1:T(8,128)(2,1)} %param.33) | copy-start | bytes 270340
  12.4 21.9 %copy-start.17 = (bf16[256,176]{0,1:T(8,128)(2,1)S(1)}, bf16[256,176]{0,1:T(8,128)(2,1)}, u32[]{:S(2)}) copy-start(bf16[256,176]{0,1:T(8,128)(2,1)} %param.32) | copy-start | bytes 270340
  12.4 22.1 %copy-start.21 = (bf16[2048]{0:T(1024)(128)(2,1)S(1)}, bf16[2048]{0:T(1024)(128)(2,1)}, u32[]{:S(2)}) copy-start(bf16[2048]{0:T(1024)(128)(2,1)} %param.30) | copy-start | bytes 12292
  13.1 9.3 %all-to-all-start = ((bf16[8,32,256]{2,1,0:T(8,128)(2,1)}), bf16[8,32,256]{2,1,0:T(8,128)(2,1)S(1)}, u32[]{:S(2)}, u32[]{:S(2)}) async-start(bf16[8,32,256]{2,1,0:T(8,128)(2,1)} %bitcast.126), calls=%async_computation | async-start | bytes 262144 | tf_op jit(solution)/shard_map/all_to_all | solution.py:15
  18.4 33.5 %copy-start.14 = (pred[32,32]{1,0:T(8,128)(4,1)}, pred[32,32]{1,0:T(8,128)(4,1)S(1)}, u32[]{:S(2)}) copy-start(pred[32,32]{1,0:T(8,128)(4,1)S(1)} %fusion.73) | copy-start | bytes 3076
  18.5 0.5 copy-start.22
  18.5 33.4 %copy-start.8 = (s32[32,32]{1,0:T(8,128)}, s32[32,32]{1,0:T(8,128)S(1)}, u32[]{:S(2)}) copy-start(s32[32,32]{1,0:T(8,128)S(1)} %reduce_window_sum.11) | copy-start | bytes 12292
  22.4 1.2 copy-start.6
  23.6 28.3 %all-to-all-start.1 = ((bf16[32,32,256]{2,1,0:T(8,128)(2,1)}), bf16[32,32,256]{2,1,0:T(8,128)(2,1)S(1)}, u32[]{:S(2)}, u32[]{:S(2)}) async-start(bf16[32,32,256]{2,1,0:T(8,128)(2,1)} %bitcast.15), calls=%async_computation.1 | async-start | bytes 1048576 | tf_op jit(solution)/shard_map/all_to_all | solution.py:15
  34.4 22.8 %collective-permute-start = (bf16[352,256]{1,0:T(8,128)(2,1)S(1)}, bf16[352,256]{1,0:T(8,128)(2,1)}, u32[]{:S(2)}, u32[]{:S(2)}) collective-permute-start(bf16[352,256]{1,0:T(8,128)(2,1)S(1)} %pad_maximum_fusion.6), channel_id=1, source_target_pairs={{0,1},{1,0},{2,3},{3,2},{4,5},{5,4},{6,7},{7,6},{8,9},{9,8},{10,11... | collective-permute-start | bytes 540680 | tf_op jit(solution)/shard_map/ppermute | solution.py:19
  51.9 3.4 %collective-permute-start.1 = (bf16[512,256]{1,0:T(8,128)(2,1)S(1)}, bf16[512,256]{1,0:T(8,128)(2,1)}, u32[]{:S(2)}, u32[]{:S(2)}) collective-permute-start(bf16[512,256]{1,0:T(8,128)(2,1)S(1)} %get-tuple-element.13), channel_id=1, source_target_pairs={{0,1},{1,0},{2,3},{3,2},{4,5},{5,4},{6,7},{7,6},{8,9},{9,8},{10,11... | collective-permute-start | bytes 786440 | tf_op jit(solution)/shard_map/ppermute | solution.py:19
  53.4 1.5 %collective-permute-start.2 = (bf16[128,256]{1,0:T(8,128)(2,1)S(1)}, bf16[128,256]{1,0:T(8,128)(2,1)S(1)}, u32[]{:S(2)}, u32[]{:S(2)}) collective-permute-start(bf16[128,256]{1,0:T(8,128)(2,1)S(1)} %reshape.434), channel_id=1, source_target_pairs={{0,1},{1,0},{2,3},{3,2},{4,5},{5,4},{6,7},{7,6},{8,9},{9,8},{10,11... | collective-permute-start | bytes 196616 | tf_op jit(solution)/shard_map/ppermute | solution.py:19
  57.2 1.9 %copy-start.20 = (bf16[7,4,128]{2,0,1:T(8,128)(2,1)S(1)}, bf16[7,4,128]{2,0,1:T(8,128)(2,1)}, u32[]{:S(2)}) copy-start(bf16[7,4,128]{2,0,1:T(8,128)(2,1)} %fusion.92) | copy-start | bytes 21508
  60.2 17.7 %all-to-all-start.2 = ((bf16[4,872,128]{2,1,0:T(8,128)(2,1)}), bf16[4,872,128]{2,1,0:T(8,128)(2,1)S(1)}, u32[]{:S(2)}, u32[]{:S(2)}) async-start(bf16[4,872,128]{2,1,0:T(8,128)(2,1)} %pad_maximum_fusion), calls=%async_computation.2 | async-start | bytes 1785856 | tf_op jit(solution)/shard_map/all_to_all | solution.py:15
  77.9 0.8 copy-start.2
  83.8 1.7 %copy-start.3 = (f32[360,128]{1,0:T(8,128)S(1)}, f32[360,128]{1,0:T(8,128)}, u32[]{:S(2)}) copy-start(f32[360,128]{1,0:T(8,128)} %copy-done.2) | copy-start | bytes 552964
  83.8 1.7 %copy-start.26 = (f32[128]{0:T(128)S(1)}, f32[128]{0:T(128)}, u32[]{:S(2)}) copy-start(f32[128]{0:T(128)} %get-tuple-element.14) | copy-start | bytes 1540
  83.8 1.7 %copy-start.27 = (f32[128]{0:T(128)S(1)}, f32[128]{0:T(128)}, u32[]{:S(2)}) copy-start(f32[128]{0:T(128)} %get-tuple-element.15) | copy-start | bytes 1540
  85.4 1.7 %collective-permute-start.3 = (bf16[128,4,256]{2,0,1:T(8,128)(2,1)S(1)}, bf16[128,4,256]{2,0,1:T(8,128)(2,1)S(1)}, u32[]{:S(2)}, u32[]{:S(2)}) collective-permute-start(bf16[128,4,256]{2,0,1:T(8,128)(2,1)S(1)} %bitcast.139), channel_id=1, source_target_pairs={{0,1},{1,0},{2,3},{3,2},{4,5},{5,4},{6,7},{7,6},{8,9},{9,8},{10,11... | collective-permute-start | bytes 786440 | tf_op jit(solution)/shard_map/ppermute | solution.py:19
  85.6 1.5 %collective-permute-start.4 = (bf16[176,128]{1,0:T(8,128)(2,1)S(1)}, bf16[176,128]{1,0:T(8,128)(2,1)S(1)}, u32[]{:S(2)}, u32[]{:S(2)}) collective-permute-start(bf16[176,128]{1,0:T(8,128)(2,1)S(1)} %fusion.62), channel_id=1, source_target_pairs={{0,1},{1,0},{2,3},{3,2},{4,5},{5,4},{6,7},{7,6},{8,9},{9,8},{10,11... | collective-permute-start | bytes 135176 | tf_op jit(solution)/shard_map/ppermute | solution.py:19
  87.4 14.3 %copy-start.18 = (bf16[176,256]{1,0:T(8,128)(2,1)S(1)}, bf16[176,256]{1,0:T(8,128)(2,1)}, u32[]{:S(2)}) copy-start(bf16[176,256]{1,0:T(8,128)(2,1)} %param.34) | copy-start | bytes 270340
  101.7 6.1 %copy-start.28 = (bf16[32,2]{0,1:T(2,128)(2,1)S(1)}, bf16[32,2]{0,1:T(2,128)(2,1)}, u32[]{:S(2)}) copy-start(bf16[32,2]{0,1:T(2,128)(2,1)} %param.36) | copy-start | bytes 388
  101.7 6.1 %copy-start.11 = (f32[32,1,64]{2,0,1:T(8,128)S(1)}, f32[32,1,64]{2,0,1:T(8,128)}, u32[]{:S(2)}) copy-start(f32[32,1,64]{2,0,1:T(8,128)} %copy-done.10) | copy-start | bytes 24580
  101.7 6.1 %copy-start.13 = (f32[32,1,64]{2,0,1:T(8,128)S(1)}, f32[32,1,64]{2,0,1:T(8,128)}, u32[]{:S(2)}) copy-start(f32[32,1,64]{2,0,1:T(8,128)} %copy-done.12) | copy-start | bytes 24580
  101.7 6.2 %copy-start.25 = (s32[32,2]{0,1:T(2,128)S(1)}, s32[32,2]{0,1:T(2,128)}, u32[]{:S(2)}) copy-start(s32[32,2]{0,1:T(2,128)} %param.35) | copy-start | bytes 772
  101.7 6.3 %copy-start.9 = (s32[32,32]{1,0:T(8,128)S(1)}, s32[32,32]{1,0:T(8,128)}, u32[]{:S(2)}) copy-start(s32[32,32]{1,0:T(8,128)} %copy-done.8) | copy-start | bytes 12292
  101.7 6.3 %copy-start.15 = (pred[32,32]{1,0:T(8,128)(4,1)S(1)}, pred[32,32]{1,0:T(8,128)(4,1)}, u32[]{:S(2)}) copy-start(pred[32,32]{1,0:T(8,128)(4,1)} %copy-done.14) | copy-start | bytes 3076
  101.8 6.3 %copy-start.23 = (s32[32]{0:T(128)S(1)}, s32[32]{0:T(128)}, u32[]{:S(2)}) copy-start(s32[32]{0:T(128)} %copy-done.22) | copy-start | bytes 388
  101.8 6.5 %copy-start.19 = (f32[32,128]{1,0:T(8,128)S(1)}, f32[32,128]{1,0:T(8,128)}, u32[]{:S(2)}) copy-start(f32[32,128]{1,0:T(8,128)} %get-tuple-element.28) | copy-start | bytes 49156
  103.1 23.3 %all-to-all-start.4 = ((bf16[32,72,128]{2,1,0:T(8,128)(2,1)}), bf16[32,72,128]{2,1,0:T(8,128)(2,1)S(1)}, u32[]{:S(2)}, u32[]{:S(2)}) async-start(bf16[32,72,128]{2,1,0:T(8,128)(2,1)} %pad_maximum_fusion.2), calls=%async_computation.4 | async-start | bytes 1179648 | tf_op jit(solution)/shard_map/all_to_all | solution.py:15
  108.3 19.1 %copy-start.7 = (f32[32,256]{1,0:T(8,128)S(1)}, f32[32,256]{1,0:T(8,128)}, u32[]{:S(2)}) copy-start(f32[32,256]{1,0:T(8,128)} %copy-done.6) | copy-start | bytes 98308
